TPU v7x, 512 devices: a whole 4x4x16 slice. The times are simulated.
512 devices in a mesh: dp: 4 (over x), kv: 64 (over z, y), tp: 2 (over core).
Axes of the slice: x: 4, y: 4, z: 16, core: 2. Of those that a mesh axis runs over, the one named last changes fastest.
Arguments:
- tokens: bfloat16 [256, 2048], P('dp', 'kv'), may hold values from -6 to 6
- w_qdown: bfloat16 [2048, 768], P('kv'), may hold values from -0.125 to 0.125
- w_kvdown: bfloat16 [2048, 512], P('kv'), may hold values from -0.125 to 0.125
- w_krope: bfloat16 [2048, 32], P('kv'), may hold values from -0.125 to 0.125
- q_gain: bfloat16 [768], replicated, may hold values from 0.099609375 to 1.8984375
- kv_gain: bfloat16 [512], replicated, may hold values from 0.099609375 to 1.8984375
- w_qup: bfloat16 [768, 16, 96], P(None, 'tp'), may hold values from -0.21875 to 0.21875
- w_kup: bfloat16 [512, 16, 64], P(None, 'tp'), may hold values from -0.25 to 0.25
- w_vup: bfloat16 [512, 16, 64], P(None, 'tp'), may hold values from -0.25 to 0.25
- out_gain: bfloat16 [1024], P('tp'), may hold values from 0.099609375 to 1.8984375
- w_out: bfloat16 [1024, 2048], P('tp', 'kv'), may hold values from -0.1875 to 0.1875
- cache_latent: bfloat16 [16, 2048, 512], P('dp', 'kv'), may hold values from -600 to 600
- cache_rope: bfloat16 [16, 2048, 32], P('dp', 'kv'), may hold values from -6 to 6
- lengths: int32 [16], P('dp'), may hold values from 1984 to 2016
- accepted: int32 [16], P('dp'), may hold values from 0 to 16
- parent: int32 [16, 16], P('dp'), may hold values from -1 to 14, as said below
Outputs:
- mixed: bfloat16 [256, 2048], P('dp', 'kv')
- latent_out: bfloat16 [16, 2048, 512], P('dp', 'kv')
- rope_out: bfloat16 [16, 2048, 32], P('dp', 'kv')
Inputs may be any that keep to these rules, and one draw needn't show every extreme that they name: parent[s, 0] = -1 and 0 <= parent[s, i] < i for i >= 1.
All inputs are finite; a program needn't handle non-finite values.
Results may differ from a plain program's by a relative error of at most 0.0165.
The roundings to bfloat16 on the way count: a program that leaves them out, or rounds other values in their place, can miss the bound.
Values may be sent and summed in bfloat16 or wider, within the bound.
No kernel may reach another device: no remote copies, remote signals or barrier semaphores. Data moves between devices by JAX's collectives and lax.ppermute only.
A program may use at most 64 MiB of HBM per device.

v0:
```python
import math

import jax
import jax.numpy as jnp
from jax import lax
from jax.sharding import Mesh
from jax.sharding import PartitionSpec as P

HEADS = 16
NOPE = 64
ROPE = 32
V_DIM = 64
KV = ("kv_0", "kv_1")


rope_base = 10000.0
epsilon = 1e-06


def in_blocks(shard, dim, peers):
    shape = shard.shape
    parts = shard.reshape(*shape[:dim], peers, shape[dim] // peers, *shape[dim + 1 :])
    return jnp.moveaxis(parts, dim, 0)


def sent_and_summed(shard, axis, dim):
    peers = lax.axis_size(axis)
    parts = lax.all_to_all(in_blocks(shard, dim, peers), axis, 0, 0, tiled=True)
    return jnp.sum(parts, axis=0)


def in_one_piece(arrays, axis, dim, along):
    both = jnp.concatenate(arrays, axis=along)
    result, at, outs = (sent_and_summed(both, axis, dim), 0, [])
    for a in arrays:
        outs.append(lax.slice_in_dim(result, at, at + a.shape[along], axis=along))
        at += a.shape[along]
    return tuple(outs)


def side_by_side(arrays, axis, dim, along):
    widths = [math.prod(a.shape[along:]) for a in arrays]
    both = jnp.concatenate(
        [a.reshape(*a.shape[:along], w) for a, w in zip(arrays, widths)], axis=along
    )
    result = lax.all_gather(both, axis, axis=dim, tiled=True)
    parts = jnp.split(result, [sum(widths[:k]) for k in range(1, len(widths))], axis=along)
    return tuple(
        (b.reshape(*result.shape[:along], *a.shape[along:]) for a, b in zip(arrays, parts))
    )


def gathered_once(shard, axis):
    leaves = jax.tree.leaves(shard)
    turns = sorted(range(len(leaves)), key=lambda k: -leaves[k].size)
    width = (1, *leaves[turns[0]].shape)[-1]
    lines = [
        jnp.pad(leaves[k].reshape(-1), (0, -leaves[k].size % width)).reshape(-1, width)
        for k in turns
    ]
    both, at, found = (lax.all_gather(jnp.concatenate(lines), axis), 0, {})
    for k, line in zip(turns, lines):
        piece = both[:, at : at + len(line)].reshape(len(both), -1)
        found[k] = piece[:, : leaves[k].size].reshape(-1, *leaves[k].shape)
        at += len(line)
    numbers = iter(range(len(leaves)))
    return jax.tree.map(lambda _: found[next(numbers)], shard)


def combined_by_axis(shard, axes, combine):
    for axis in axes:
        pieces = gathered_once(shard, axis)
        shard = jax.tree.map(lambda part: part[0], pieces)
        for k in range(1, lax.axis_size(axis)):
            shard = combine(shard, jax.tree.map(lambda part: part[k], pieces))
    return shard


def copy_for_each(shard, axis):
    peers = lax.axis_size(axis)
    return lax.all_to_all(
        jnp.broadcast_to(shard[None], (peers, *shard.shape)), axis, 0, 0, tiled=True
    )


def of_everyone(shard, axis):
    everything = copy_for_each(shard, axis)
    return jnp.sum(everything, axis=0)


def in_one(arrays, axis):
    ends = [0]
    for a in arrays:
        ends.append(ends[-1] + a.size)
    total = of_everyone(jnp.concatenate([a.ravel() for a in arrays]), axis)
    return tuple((total[b:e].reshape(a.shape) for a, b, e in zip(arrays, ends, ends[1:])))


def rotate(vector, positions):
    half_size = vector.shape[-1] // 2
    frequency = rope_base ** (-jnp.arange(half_size, dtype=jnp.float32) / half_size)
    angles = positions[..., None] * frequency
    cosine = jnp.cos(angles)
    sine_part = jnp.sin(angles)
    first_half = vector[..., :half_size]
    second_half = vector[..., half_size:]
    return jnp.concatenate(
        [
            first_half * cosine - second_half * sine_part,
            second_half * cosine + first_half * sine_part,
        ],
        axis=-1,
    )


def normalize(vector, gain):
    return (
        vector
        * lax.rsqrt(jnp.mean(vector * vector, axis=-1, keepdims=True) + epsilon)
        * gain.astype(jnp.float32)
    )


def ancestry(parent):
    proposals = parent.shape[-1]
    column = jnp.arange(proposals, dtype=jnp.int32)
    single = (parent[:, :, None] == column[None, None, :]).astype(jnp.float32)
    reached = jnp.minimum(single + jnp.eye(proposals, dtype=jnp.float32), 1.0)
    for repeat in range(max((proposals - 1).bit_length(), 1)):
        reached = jnp.minimum(jnp.einsum("sij,sjk->sik", reached, reached), 1.0)
    depths = jnp.sum(reached, axis=-1) - 1.0
    return (reached, depths)


def prepare(q_latent, kv_latent, rope_raw, positions, q_gain, kv_gain, w_qup):
    q_normed = normalize(q_latent, q_gain).astype(jnp.bfloat16)
    new_latent = normalize(kv_latent, kv_gain).astype(jnp.bfloat16)
    new_rope = rotate(rope_raw, positions).astype(jnp.bfloat16)
    query = jnp.einsum("tr,rhd->thd", q_normed, w_qup, preferred_element_type=jnp.float32)
    query_full = jnp.concatenate(
        [query[..., :NOPE], rotate(query[..., NOPE:], positions[:, None])], axis=-1
    ).astype(jnp.bfloat16)
    return (query_full, new_latent, new_rope)


def partial_attention(q_absorbed, q_rotary, latent, rotary, allowed):
    scores = (
        jnp.einsum("sphr,skr->sphk", q_absorbed, latent, preferred_element_type=jnp.float32)
        + jnp.einsum("sphd,skd->sphk", q_rotary, rotary, preferred_element_type=jnp.float32)
    ) * (NOPE + ROPE) ** (-0.5)
    masked = jnp.where(allowed, scores, -1e30)
    peak = jnp.max(masked, axis=-1)
    weights = jnp.where(allowed, jnp.exp(masked - peak[..., None]), 0.0)
    mass = jnp.sum(weights, axis=-1)
    blend = jnp.einsum(
        "sphk,skr->sphr", weights.astype(jnp.bfloat16), latent, preferred_element_type=jnp.float32
    )
    return (peak, mass, blend)


def combine(earlier, later):
    peak_first, mass_first, blend_first = earlier
    peak_second, mass_second, blend_second = later
    peak = jnp.maximum(peak_first, peak_second)
    scale_first = jnp.exp(peak_first - peak)
    scale_second = jnp.exp(peak_second - peak)
    return (
        peak,
        mass_first * scale_first + mass_second * scale_second,
        blend_first * scale_first[..., None] + blend_second * scale_second[..., None],
    )


def to_values(blend, w_vup):
    return jnp.einsum("sphr,rhv->sphv", blend, w_vup.astype(jnp.float32))


def shards(
    tokens,
    w_qdown,
    w_kvdown,
    w_krope,
    q_gain,
    kv_gain,
    w_qup,
    w_kup,
    w_vup,
    out_gain,
    w_out,
    cache_latent,
    cache_rope,
    lengths,
    accepted,
    parent,
):
    seq_count, proposals = parent.shape
    local_heads = w_qup.shape[1]
    tok_count = tokens.shape[0]
    q_part = jnp.dot(tokens, w_qdown, preferred_element_type=jnp.float32)
    kv_part = jnp.dot(tokens, w_kvdown, preferred_element_type=jnp.float32)
    rope_part = jnp.dot(tokens, w_krope, preferred_element_type=jnp.float32)
    reached, depths = ancestry(parent)
    valid = lengths + accepted
    positions = (valid[:, None].astype(jnp.float32) + depths).reshape(-1)
    share = tok_count // lax.axis_size(KV)
    q_latent, kv_latent, rope_raw = in_one_piece((q_part, kv_part, rope_part), KV, 0, 1)
    own_positions = lax.dynamic_slice_in_dim(positions, lax.axis_index(KV) * share, share)
    piece_query, piece_latent, piece_rope = prepare(
        q_latent, kv_latent, rope_raw, own_positions, q_gain, kv_gain, w_qup
    )
    query_full, new_latent, new_rope = side_by_side(
        (piece_query, piece_latent, piece_rope), KV, 0, 1
    )
    q_rotary = query_full[..., NOPE:].reshape(seq_count, proposals, local_heads, -1)
    q_absorbed = jnp.einsum(
        "thn,rhn->thr", query_full[..., :NOPE], w_kup, preferred_element_type=jnp.float32
    )
    q_absorbed = q_absorbed.astype(jnp.bfloat16).reshape(seq_count, proposals, local_heads, -1)
    pos_count = cache_latent.shape[1]
    key_pos = lax.axis_index(KV) * pos_count + jnp.arange(pos_count, dtype=jnp.int32)
    visible = (key_pos[None, :] < valid[:, None])[:, None, None, :]
    own_latent = new_latent.reshape(seq_count, proposals, -1)
    own_rope = new_rope.reshape(seq_count, proposals, -1)
    peak_cache, mass_cache, blend_cache = partial_attention(
        q_absorbed, q_rotary, cache_latent, cache_rope, visible
    )
    peak_own, mass_own, blend_own = partial_attention(
        q_absorbed, q_rotary, own_latent, own_rope, (reached > 0.5)[:, :, None, :]
    )
    merged = combined_by_axis((peak_cache, mass_cache, to_values(blend_cache, w_vup)), KV, combine)
    peak, mass, blend = combine(merged, (peak_own, mass_own, to_values(blend_own, w_vup)))
    head_values = blend / mass[..., None]
    flat_values = head_values.reshape(tok_count, -1)
    squares = jnp.sum(flat_values * flat_values, axis=-1)
    scaled = (flat_values * out_gain.astype(jnp.float32)).astype(jnp.bfloat16)
    partial_value = jnp.dot(scaled, w_out, preferred_element_type=jnp.float32)
    summed, square_sum = in_one((partial_value, squares), "tp")
    mixed = (summed * lax.rsqrt(square_sum[:, None] / (HEADS * V_DIM) + epsilon)).astype(
        jnp.bfloat16
    )
    targets = valid[:, None] + jnp.arange(proposals, dtype=jnp.int32)[None, :]
    hits = key_pos[None, :, None] == targets[:, None, :]
    hit_table = hits.astype(jnp.bfloat16)
    used = jnp.any(hits, axis=-1)[..., None]
    placed_latent = jnp.einsum(
        "skp,spr->skr", hit_table, own_latent, preferred_element_type=jnp.float32
    ).astype(jnp.bfloat16)
    placed_rope = jnp.einsum(
        "skp,spr->skr", hit_table, own_rope, preferred_element_type=jnp.float32
    ).astype(jnp.bfloat16)
    latent_out = jnp.where(used, placed_latent, cache_latent)
    rope_out = jnp.where(used, placed_rope, cache_rope)
    return (mixed, latent_out, rope_out)


def solution(mesh):
    finer = Mesh(
        mesh.devices.reshape(mesh.shape["dp"], 16, 4, mesh.shape["tp"]),
        ("dp", "kv_0", "kv_1", "tp"),
    )
    in_specs = (
        P("dp", KV),
        P(KV, None),
        P(KV, None),
        P(KV, None),
        P(),
        P(),
        P(None, "tp", None),
        P(None, "tp", None),
        P(None, "tp", None),
        P("tp"),
        P("tp", KV),
        P("dp", KV, None),
        P("dp", KV, None),
        P("dp"),
        P("dp"),
        P("dp", None),
    )
    out_specs = (P("dp", KV), P("dp", KV, None), P("dp", KV, None))
    return jax.shard_map(
        shards, mesh=finer, in_specs=in_specs, out_specs=out_specs, check_vma=False
    )
```

profile of v0, /device:TPU:1, one launch (start us, length us, event | category | flops | bytes accessed | tf_op | source)
XLA Modules:
  0.0 263.7 jit_solution(6085995971741213386)
XLA Ops:
  7.2 1.0 fusion.224
  8.2 0.9 fusion.223
  9.2 1.0 fusion.222
  10.2 1.1 copy.404
  11.3 19.4 %all-to-all-start = ((f32[64,1,1312]{2,1,0:T(1,128)}), f32[64,1,1312]{2,1,0:T(1,128)S(1)}, u32[]{:S(2)}, u32[]{:S(2)}) async-start(f32[64,1,1312]{2,1,0:T(1,128)} %copy.404), calls=%async_computation | async-start | bytes 720896 | tf_op jit(solution)/shard_map/all_to_all | solution.py:28
  30.9 0.3 convolution_minimum_fusion.2
  31.2 0.3 fusion.217
  31.7 0.6 dynamic_slice.3
  32.3 0.7 fusion.205
  33.1 21.4 %all-to-all-done = f32[64,1,1312]{2,1,0:T(1,128)S(1)} async-done(((f32[64,1,1312]{2,1,0:T(1,128)}), f32[64,1,1312]{2,1,0:T(1,128)S(1)}, u32[]{:S(2)}, u32[]{:S(2)}) %all-to-all-start) | async-done | bytes 335904 | tf_op jit(solution)/shard_map/all_to_all | solution.py:28
  54.5 0.2 reduce_sum.76
  54.8 0.6 multiply_reduce_fusion.2
  55.4 0.6 multiply_reduce_fusion.1
  56.0 0.7 add_convert_fusion.1
  58.1 0.5 fusion.192
  59.0 69.5 %all-gather.2 = bf16[64,1,1312]{2,1,0:T(2,128)(2,1)S(1)} all-gather(bf16[1,1,1312]{2,1,0:T(2,128)(2,1)S(1)} %bitcast.667), channel_id=1, replica_groups=mesh['dp'=4,'kv_0'=16,'kv_1'=4,'tp'=2] {'kv_0','kv_1'}, dimensions={0}, use_global_device_ids=true | all-gather | bytes 170560 | tf_op jit(solution)/shard_map/all_gather | solution.py:46
  128.5 0.2 reshape.1634
  128.7 0.1 slice.430
  128.8 0.3 convolution_convert_fusion
  129.1 0.4 fusion.31
  129.5 0.3 fusion.218
  129.9 0.3 fusion.40
  130.3 0.5 fusion.6
  130.8 0.2 copy.412
  130.9 0.8 copy.413
  131.9 0.1 compare_reduce_fusion
  132.0 0.4 fusion.29
  132.4 0.3 fusion.219
  132.8 0.3 fusion.41
  133.1 0.9 fusion.26
  134.0 1.0 fusion.25
  134.9 81.7 %all-gather.7.cloned.1.call-done = f32[16,528,64]{1,2,0:T(8,128)} async-done(((f32[1,528,64]{1,2,0:T(8,128)}), f32[16,528,64]{1,2,0:T(8,128)}) %all-gather.7.cloned.1.call-update) | async-done | bytes 2162704 | tf_op jit(solution)/shard_map/all_gather | solution.py:61
  216.6 1.2 fusion.213
  220.2 1.1 fusion.214
  222.4 0.1 fusion.121
  222.8 1.9 fusion.44
  224.8 10.4 %all-gather.4 = f32[4,528,64]{1,2,0:T(8,128)S(1)} all-gather(f32[1,528,64]{1,2,0:T(8,128)S(1)} %maximum_bitcast_fusion.2), channel_id=3, replica_groups=mesh['dp'=4,'kv_0'=16,'kv_1'=4,'tp'=2] {'kv_1'}, dimensions={0}, use_global_device_ids=true | all-gather | bytes 675840 | tf_op jit(solution)/shard_map/all_gather | solution.py:61
  236.0 0.1 copy.489
  237.3 0.1 copy.545
  237.5 0.1 copy.547
  237.6 0.1 copy.546
  237.7 0.1 copy.548
  237.9 0.9 multiply_reduce_fusion
  238.9 0.2 copy.492
  239.1 0.1 reshape.1642
  239.2 0.1 fusion.96
  239.4 16.5 %all_to_all.11 = f32[2,1,2112]{2,1,0:T(1,128)S(1)} all-to-all(f32[2,1,2112]{2,1,0:T(1,128)S(1)} %broadcast_in_dim.68), channel_id=1, replica_groups=mesh['dp'=4,'kv_0'=16,'kv_1'=4,'tp'=2] {'tp'}, dimensions={0} | all-to-all | bytes 33792 | tf_op jit(solution)/shard_map/all_to_all | solution.py:81
  256.2 0.7 copy.495
  (158 shorter events, 7.1 us)
Async XLA Ops:
  7.2 50.9 %copy-start = (bf16[768,8,96]{0,2,1:T(8,128)(2,1)S(1)}, bf16[768,8,96]{0,2,1:T(8,128)(2,1)}, u32[]{:S(2)}) copy-start(bf16[768,8,96]{0,2,1:T(8,128)(2,1)} %param.22) | copy-start | bytes 3538948
  7.2 23.6 %copy-start.7 = (bf16[512]{0:T(512)(128)(2,1)S(1)}, bf16[512]{0:T(512)(128)(2,1)}, u32[]{:S(2)}) copy-start(bf16[512]{0:T(512)(128)(2,1)} %param.21) | copy-start | bytes 3076
  7.2 23.6 %copy-start.6 = (bf16[768]{0:T(1024)(128)(2,1)S(1)}, bf16[768]{0:T(1024)(128)(2,1)}, u32[]{:S(2)}) copy-start(bf16[768]{0:T(1024)(128)(2,1)} %param.20) | copy-start | bytes 4612
  7.2 23.7 %copy-start.10 = (s32[4]{0:T(128)S(1)}, s32[4]{0:T(128)}, u32[]{:S(2)}) copy-start(s32[4]{0:T(128)} %param.30) | copy-start | bytes 52
  7.2 23.7 %copy-start.9 = (s32[4]{0:T(128)S(1)}, s32[4]{0:T(128)}, u32[]{:S(2)}) copy-start(s32[4]{0:T(128)} %param.29) | copy-start | bytes 52
  7.2 23.7 %copy-start.11 = (s32[4,16]{1,0:T(4,128)S(1)}, s32[4,16]{1,0:T(4,128)}, u32[]{:S(2)}) copy-start(s32[4,16]{1,0:T(4,128)} %param.31) | copy-start | bytes 772
  10.2 118.6 %copy-start.1 = (bf16[512,8,64]{0,2,1:T(8,128)(2,1)S(1)}, bf16[512,8,64]{0,2,1:T(8,128)(2,1)}, u32[]{:S(2)}) copy-start(bf16[512,8,64]{0,2,1:T(8,128)(2,1)} %param.23) | copy-start | bytes 1572868
  11.3 117.8 %copy-start.3 = (bf16[4,32,512]{2,1,0:T(8,128)(2,1)S(1)}, bf16[4,32,512]{2,1,0:T(8,128)(2,1)}, u32[]{:S(2)}) copy-start(bf16[4,32,512]{2,1,0:T(8,128)(2,1)} %param.27) | copy-start | bytes 393220
  11.3 43.2 %all-to-all-start = ((f32[64,1,1312]{2,1,0:T(1,128)}), f32[64,1,1312]{2,1,0:T(1,128)S(1)}, u32[]{:S(2)}, u32[]{:S(2)}) async-start(f32[64,1,1312]{2,1,0:T(1,128)} %copy.404), calls=%async_computation | async-start | bytes 720896 | tf_op jit(solution)/shard_map/all_to_all | solution.py:28
  30.7 185.9 %all-gather.7.cloned.1.call-start = ((), (), s32[]{:S(2)}) async-start(), calls=%async_computation.2 | async-start | bytes 2785280 | tf_op jit(solution)/shard_map/all_gather | solution.py:61
  33.1 96.4 %copy-start.4 = (bf16[4,32,32]{2,1,0:T(8,128)(2,1)S(1)}, bf16[4,32,32]{2,1,0:T(8,128)(2,1)}, u32[]{:S(2)}) copy-start(bf16[4,32,32]{2,1,0:T(8,128)(2,1)} %param.28) | copy-start | bytes 24580
  58.6 71.7 %copy-start.2 = (bf16[512,8,64]{0,2,1:T(8,128)(2,1)S(1)}, bf16[512,8,64]{0,2,1:T(8,128)(2,1)}, u32[]{:S(2)}) copy-start(bf16[512,8,64]{0,2,1:T(8,128)(2,1)} %param.24) | copy-start | bytes 1572868
  129.1 2.7 %copy-start.8 = (bf16[512]{0:T(512)(128)(2,1)S(1)}, bf16[512]{0:T(512)(128)(2,1)}, u32[]{:S(2)}) copy-start(bf16[512]{0:T(512)(128)(2,1)} %param.25) | copy-start | bytes 3076
  237.9 1.3 copy-start.5
Sparse Core Ops, SparseCore 0:
  131.9 84.6 all-gather.6
where the time goes:
time: 264 us
  waiting for transfers between devices  103 us (39%)
  blocking collectives  96.5 us (37%)
  starting transfers between devices  19.4 us (7%)
  between operations  16.2 us (6%)
  local copies, waits for them, and re-layouts  13 us (5%)
  matrix products  9.06 us (3%)
  other arithmetic  6.44 us (2%)
    all_gather x1, waiting for transfers between devices, gathered_once(): both, at, found = (lax.all_gather(jnp.concatenate(lines), axis), 0, {})  81.7 us
    all_gather x1, blocking collectives, side_by_side(): result = lax.all_gather(both, axis, axis=dim, tiled=True)  69.5 us
    all_to_all x1, waiting for transfers between devices, sent_and_summed(): parts = lax.all_to_all(in_blocks(shard, dim, peers), axis, 0, 0, tiled=True)  21.4 us
    all_to_all x1, starting transfers between devices, sent_and_summed(): parts = lax.all_to_all(in_blocks(shard, dim, peers), axis, 0, 0, tiled=True)  19.4 us
    all_to_all x1, blocking collectives, copy_for_each(): lax.all_to_all(jnp.broadcast_to(shard[None], (peers, *shard.shape)), axis...  16.5 us
    all_gather x1, blocking collectives, gathered_once(): both, at, found = (lax.all_gather(jnp.concatenate(lines), axis), 0, {})  10.4 us
  transfers between devices with their start and end apart: 2, of which 2 were waited for; matrix products, arithmetic and copies ran while one was open for 2% of the time, Pallas kernels for 0%

commit v1 on v0

v1 whole, which is shorter than its diff:
```python
import jax
import jax.numpy as jnp
from jax import lax
from jax.experimental import pallas as pl
from jax.experimental.pallas import tpu as pltpu
from jax.sharding import PartitionSpec as P

HEADS = 16
NOPE = 64
ROPE = 32
V_DIM = 64


FOUR = range(4)
LOWS = ((2, 3, 1, 0), (2, 3, 1, 0), (0, 1, 2, 3), (1, 0, 2, 3))
HIGHS = (2, 3, 0, 1)
YS = (2, 3, 0, 1)


def place_of(high, low, y):
    return (high * 4 + LOWS[high][low]) * 4 + YS[y]


BLOCK = [[place_of(high, low, y) for low in FOUR for y in FOUR] for high in FOUR]
RING = [[place_of(high, low, y) for high in HIGHS for low in FOUR] for y in FOUR]
ROW = [
    [place_of(high, low, y) * 2 + core for y in FOUR for core in (0, 1)]
    for high in FOUR
    for low in FOUR
]


def packed(entries):
    word = sum(entry << 2 * k for k, entry in enumerate(entries))
    return word - (1 << 32) if word >> 31 else word


def entry_of(entries, k):
    return (jnp.int32(packed(entries)) >> (2 * k)) & 3


LOW_AT = [row for lows in LOWS for row in lows]
LOW_OF = [lows.index(row) for lows in LOWS for row in FOUR]
Y_OF = [YS.index(y) for y in FOUR]


rope_base = 10000.0
epsilon = 1e-06
f32 = jnp.float32
bf16 = jnp.bfloat16
i32 = jnp.int32
TINY = -1e30


def iota(shape, dim):
    return lax.broadcasted_iota(i32, shape, dim)


def dot(a, b, precision=None):
    return lax.dot_general(
        a, b, (((1,), (0,)), ((), ())), precision=precision, preferred_element_type=f32
    )


def dot_nt(a, b):
    return lax.dot_general(a, b, (((1,), (1,)), ((), ())), preferred_element_type=f32)


def one_hot(test):
    return jnp.where(test, 1.0, 0.0).astype(bf16)


def rope_spread():
    column = iota((32, 256), 1)
    return one_hot(iota((32, 256), 0) == (column >> 7) * 16 + (column & 15))


def side_by_side(ref):
    rows = ref[...].astype(f32)
    return jnp.concatenate([rows[k : k + 1] for k in range(rows.shape[0])], axis=1)


def started(sources, copies, arrived):
    moves = [pltpu.make_async_copy(a, b, arrived.at[k]) for k, (a, b) in enumerate(zip(sources, copies))]
    for move in moves:
        move.start()
    return moves


def project_body(*refs):
    sources, (out, cosine, sine, reach), copies, arrived = refs[:9], refs[9:13], refs[13:22], refs[22]
    moves = started(sources, copies, arrived)
    for move in moves[:3]:
        move.wait()
    tables_body(*copies[:3], cosine, sine, reach)
    tokens, w_q, w_kv, w_kr, latent, rope = copies[3:]
    row = iota((128, 64), 0)
    token = ((row >> 3) & 3) * 16 + (row >> 5) * 4 + (row & 3)
    pick = one_hot(iota((128, 64), 1) == token)
    spread = rope_spread()
    for move in moves[3:]:
        move.wait()
    rows = dot_nt(pick, tokens[...]).astype(bf16)
    w_kr_spread = dot(w_kr[...], spread).astype(bf16)
    core = lax.axis_index("tp")
    w_core = jnp.where(core == 0, w_q[...], jnp.concatenate([w_kv[...], w_kr_spread], axis=1))
    part = dot(rows, w_core)
    first = ((iota((128, 1), 0) >> 2) & 1) == 0
    part = jnp.where(first, part[:, :384], part[:, 384:])
    part_high = part.astype(bf16)
    part_low = (part - part_high.astype(f32)).astype(bf16)
    out[:, :, 0:384] = part_high.reshape(16, 8, 384)
    out[:, :, 1536:1920] = part_low.reshape(16, 8, 384)
    for s in range(4):
        for g in range(4):
            span = latent[s, 8 * g : 8 * g + 8, :]
            span = jnp.where(core == 0, span[:, :256], span[:, 256:])
            key = rope[s, 8 * g : 8 * g + 8, :]
            for a in range(4):
                out[a * 4 + s, :, 384 + 256 * g : 640 + 256 * g] = span
                out[a * 4 + s, :, 1408 + 32 * g : 1440 + 32 * g] = key


def tables_body(lengths, accepted, parent, cosine, sine, reach):
    s = entry_of(Y_OF, lax.axis_index("kv") & 3)
    valid = lengths[s] + accepted[s]
    line = iota((16, 128), 0)
    masks = jnp.zeros((16, 128), i32)
    seen = []
    for i in range(16):
        mask = jnp.int32(1 << i)
        if i:
            up = parent[s, i]
            for j in range(i):
                mask = mask | jnp.where(up == j, seen[j], 0)
        seen.append(mask)
        masks = jnp.where(line == i, mask, masks)
    lane = iota((16, 128), 1)
    bits = jnp.where(lane < 16, (masks >> jnp.minimum(lane, 15)) & 1, 0).astype(f32)
    depth = jnp.sum(bits, axis=1, keepdims=True) - 1.0
    position = valid.astype(f32) + depth
    shard = lax.axis_index("kv")
    part = entry_of(LOW_OF, shard >> 2)
    row = iota((40, 16), 0)
    token = jnp.where(row < 32, row >> 3, part) * 4 + (row & 3)
    pick = jnp.where(iota((40, 16), 1) == token, 1.0, 0.0)
    spread = dot(pick, jnp.broadcast_to(position, (16, 128)), lax.Precision.HIGHEST)
    k = (iota((40, 128), 1) & 15).astype(f32)
    angle = spread * jnp.exp(k * (-9.210340371976184 / 16.0))
    cosine[...] = jnp.cos(angle)
    sine[...] = jnp.sin(angle)
    row = iota((32, 16), 0)
    pick = one_hot(iota((32, 16), 1) == part * 4 + (row & 3))
    own = jnp.where(shard < 16, dot(pick, bits.astype(bf16)), 0.0)
    lane = iota((32, 128), 1)
    for k in range(4):
        own = jnp.where(lane == 123 + k, (lengths[k] + accepted[k]).astype(f32), own)
    reach[...] = jnp.where(lane == 127, valid.astype(f32), own)


def block_sum_body(parts, out):
    same = one_hot((iota((128, 128), 0) & 7) == (iota((128, 128), 1) & 7))
    total = dot(same, parts[:, :, 0:384].reshape(128, 384))
    total += dot(same, parts[:, :, 1536:1920].reshape(128, 384))
    high = total.astype(bf16)
    low = (total - high.astype(f32)).astype(bf16)
    out[:, :, 0:384] = high.reshape(16, 8, 384)
    out[:, :, 384:768] = low.reshape(16, 8, 384)


def normalize_body(ring, block, cosine, sine, q_gain, kv_gain, w_out, out, key_rope):
    x = jnp.sum(ring[...].astype(f32).reshape(4, 32, 768), axis=0).reshape(4, 8, 768)
    x = x[:, :, 0:384] + x[:, :, 384:768]
    x = jnp.concatenate([x, pltpu.roll(x, 4, 1)], axis=2)
    part = entry_of(LOW_OF, lax.axis_index("kv") >> 2)
    query = x[3]
    for k in range(3):
        query = jnp.where(part == k, x[k], query)
    q_scale = lax.rsqrt(jnp.sum(query * query, axis=1, keepdims=True) * (1.0 / 768) + epsilon)
    q_normed = query * q_scale * side_by_side(q_gain)
    x = x.reshape(32, 768)
    left = x[:, :512]
    kv_scale = lax.rsqrt(jnp.sum(left * left, axis=1, keepdims=True) * (1.0 / 512) + epsilon)
    latents = left * kv_scale * side_by_side(kv_gain)
    cos = cosine[0:32, :]
    sin = sine[0:32, :]
    rope_1 = x[:, 512:640] * cos - x[:, 640:768] * sin
    rope_2 = x[:, 640:768] * cos + x[:, 512:640] * sin
    kv_rows = jnp.concatenate([latents, rope_1, rope_2], axis=1)
    rows = jnp.where(lax.axis_index("tp") == 0, jnp.concatenate([q_normed] * 4, axis=0), kv_rows)
    rows = rows.astype(bf16)
    for g in range(4):
        span = block[:, :, 384 + 256 * g : 640 + 256 * g]
        out[128 * g : 128 * g + 128, :] = span.reshape(128, 256)
    for k in range(3):
        out[512 + 32 * k : 544 + 32 * k, :] = rows[:, 256 * k : 256 * k + 256]
    out[608:640, :] = w_out[:, 0:256]
    out[640:672, :] = w_out[:, 256:512]
    key_rope[...] = block[:, :, 1408:1536].reshape(128, 128)


def attend_body(own, other, far_rope, cosine, sine, reach, w_q, w_k, w_v, *refs):
    caches, (out, fresh), kept, arrived = refs[:2], refs[2:4], refs[4:6], refs[6]
    moves = started(caches, kept, arrived)
    shard = lax.axis_index("kv")
    high = shard >> 4
    part = entry_of(LOW_OF, shard >> 2)
    core = lax.axis_index("tp")
    from_0 = jnp.where(core == 0, own[...], other[...])
    from_1 = jnp.where(core == 0, other[...], own[...])
    spans = [slice(512 + 32 * k, 544 + 32 * k) for k in range(3)]
    q_normed = jnp.concatenate([from_0[span][0:8] for span in spans], axis=1)
    latents = jnp.concatenate([from_1[span] for span in spans[:2]], axis=1)
    rope_1 = from_1[576:608, 0:128]
    rope_2 = from_1[576:608, 128:256]
    cos = cosine[32:40, :]
    sin = sine[32:40, :]
    spans = [(0, 64), (64, 80), (80, 96)]
    w_q = [w_q[96 * h + lo : 96 * h + hi, :] for lo, hi in spans for h in range(8)]
    query = dot_nt(q_normed, jnp.concatenate(w_q, axis=0))
    turned_1 = query[:, 512:640] * cos - query[:, 640:768] * sin
    turned_2 = query[:, 640:768] * cos + query[:, 512:640] * sin
    query = jnp.concatenate([query[:, :512], turned_1, turned_2], axis=1)
    query = jnp.where(iota((8, 1), 0) < 4, query, pltpu.roll(query, 4, 0))
    rows = jnp.broadcast_to(query[None], (4, 8, 768)).reshape(32, 768)
    row = iota((32, 768), 0)
    lane = iota((32, 768), 1)
    head = ((row >> 2) & 1) * 4 + (row >> 3)
    lane_head = jnp.where(lane < 512, lane >> 6, (lane & 127) >> 4)
    rows = jnp.where(head == lane_head, rows, 0.0).astype(bf16)
    q_abs = dot(rows[:, :512], w_k[...]).astype(bf16)
    q_rot = rows[:, 512:]
    row = iota((16, 32), 0)
    pick = one_hot(iota((16, 32), 1) == (row >> 2) * 8 + (row & 3))
    own_latent = dot(pick, latents).astype(bf16)
    own_rope = jnp.concatenate([dot(pick, rope_1), dot(pick, rope_2)], axis=1).astype(bf16)
    fresh[:, 0:512] = own_latent
    fresh[:, 512:640] = jnp.zeros((16, 128), bf16)
    fresh[:, 512:528] = own_rope[:, 0:16]
    fresh[:, 528:544] = own_rope[:, 128:144]
    keys = jnp.concatenate([from_0[0:512], from_1[0:512]], axis=1)
    lane = iota((128, 256), 0)
    column = iota((128, 256), 1)
    entry = (column >> 7) * 16 + (column & 15)
    key_rope = jnp.concatenate(
        [dot(far_rope[...], one_hot(lane == 32 * g + entry)) for g in range(4)], axis=0
    ).astype(bf16)
    scale = (NOPE + ROPE) ** (-0.5)
    score = (dot_nt(q_abs, keys) + dot_nt(q_rot, key_rope)) * scale
    own_score = (dot_nt(q_abs, own_latent) + dot_nt(q_rot, own_rope)) * scale
    key = iota((32, 512), 1)
    source = high * 4 + entry_of(LOW_AT, high * 4 + ((key >> 5) & 3))
    place = (source * 4 + entry_of(YS, (key >> 3) & 3)) * 32 + (key >> 7) * 8 + (key & 7)
    seen = place < reach[:, 127:128].astype(i32)
    own_seen = reach[:, 0:16] > 0.5
    score = jnp.where(seen, score, TINY)
    own_score = jnp.where(own_seen, own_score, TINY)
    top = jnp.maximum(
        jnp.max(score, axis=1, keepdims=True), jnp.max(own_score, axis=1, keepdims=True)
    )
    weight = jnp.where(seen, jnp.exp(score - top), 0.0)
    own_weight = jnp.where(own_seen, jnp.exp(own_score - top), 0.0)
    mass = jnp.sum(weight, axis=1, keepdims=True) + jnp.sum(own_weight, axis=1, keepdims=True)
    blend = dot(weight.astype(bf16), keys) + dot(own_weight.astype(bf16), own_latent)
    blend_high = blend.astype(bf16)
    blend_low = (blend - blend_high.astype(f32)).astype(bf16)
    value = dot_nt(jnp.concatenate([blend_high, blend_low], axis=0), w_v[...])
    value = (value[:32] + value[32:]) / jnp.maximum(mass, 1e-30)
    row = iota((32, 512), 0)
    head = ((row >> 2) & 1) * 4 + (row >> 3)
    value = jnp.where(head == iota((32, 512), 1) >> 6, value, 0.0)
    value = jnp.sum(value.reshape(4, 8, 512), axis=0)
    value = (value + pltpu.roll(value, 4, 0))[0:4].astype(bf16)
    out[:, :, 0:512] = jnp.broadcast_to(value[None], (16, 4, 512))
    mass_log = jnp.where(mass > 0, top + jnp.log(jnp.maximum(mass, 1e-30)), TINY)
    row = iota((32, 128), 0)
    lane = iota((32, 128), 1)
    head = ((row >> 2) & 1) * 4 + (row >> 3)
    mass_log = jnp.where((head == (lane & 7)) & (lane < 24), mass_log, 0.0)
    mass_log = jnp.sum(mass_log.reshape(4, 8, 128), axis=0)
    terms = three_terms(mass_log + pltpu.roll(mass_log, 4, 0))[0:4]
    out[:, :, 512:640] = jnp.broadcast_to(terms[None], (16, 4, 128))
    for move in moves:
        move.wait()


def three_terms(rows):
    high = rows.astype(bf16).astype(f32)
    middle = (rows - high).astype(bf16).astype(f32)
    low = rows - high - middle
    lane = iota(rows.shape, 1)
    terms = jnp.where(lane < 8, high, jnp.where(lane < 16, middle, jnp.where(lane < 24, low, 0.0)))
    return terms.astype(bf16)


def flat_body(parts, fresh, out_gain, out):
    rows = jnp.concatenate([parts[k].astype(f32) for k in range(16)], axis=0)
    lane = iota((128, 512), 0)
    spread = one_hot(((lane & 7) == iota((128, 512), 1) >> 6) & (lane < 24))
    mass_log = dot(rows[:, 512:640].astype(bf16), spread).reshape(4, 16, 512)
    weight = jnp.exp(mass_log - jnp.max(mass_log, axis=0, keepdims=True))
    value = jnp.sum(weight * rows[:, 0:512].reshape(4, 16, 512), axis=0)
    value = value / jnp.sum(weight, axis=0)
    square = jnp.sum(value * value, axis=1, keepdims=True)
    scaled = (value * side_by_side(out_gain)).astype(bf16)
    high = square.astype(bf16).astype(f32)
    middle = (square - high).astype(bf16).astype(f32)
    low = square - high - middle
    lane = iota((16, 128), 1)
    tail = fresh[:, 512:640].astype(f32)
    tail = jnp.where(lane == 32, high, jnp.where(lane == 33, middle, tail))
    tail = jnp.where(lane == 34, low, tail).astype(bf16)
    half = jnp.where(lax.axis_index("tp") == 0, fresh[:, 0:256], fresh[:, 256:512])
    out[:, :, 0:512] = jnp.broadcast_to(scaled[None], (8, 16, 512))
    out[:, :, 512:768] = jnp.broadcast_to(half[None], (8, 16, 256))
    out[:, :, 768:896] = jnp.broadcast_to(tail[None], (8, 16, 128))


def output_body(parts, own, other, reach, latent, rope, *refs):
    (out, *outs), (latent_new, rope_new, arrived) = refs[2:5], refs[5:]
    core = lax.axis_index("tp")
    lane = iota((8, 128), 1)
    terms = one_hot((lane >= 32) & (lane < 35))
    weights = [jnp.concatenate([r[608:640, :], r[640:672, :]], axis=1) for r in (own, other)]
    product = square = 0.0
    for c in range(2):
        chunk = jnp.concatenate([parts[2 * s + c] for s in range(4)], axis=0)
        weight = jnp.where(core == c, weights[0], weights[1])
        product += dot_nt(weight, chunk[:, 0:512])
        square += dot_nt(terms, chunk[:, 768:896])
    scale = lax.rsqrt(square[0:1] * (1.0 / (HEADS * V_DIM)) + epsilon)
    out[...] = (product * scale).astype(bf16)
    shard = lax.axis_index("kv")

    @pl.when(shard >= 62)
    def _():
        place = shard * 32 + iota((32, 16), 0)
        for s in range(4):
            valid = reach[:, 123 + s : 124 + s].astype(i32)
            hit = one_hot(place == valid + iota((32, 16), 1))
            used = jnp.sum(hit.astype(f32), axis=1, keepdims=True) > 0.5
            new = jnp.concatenate([parts[2 * s + c, :, 512:768] for c in range(2)], axis=1)
            latent_new[s] = jnp.where(used, dot(hit, new), latent[s].astype(f32)).astype(bf16)
            placed = dot(hit, parts[2 * s, :, 768:896])[:, 0:32]
            rope_new[s] = jnp.where(used, placed, rope[s].astype(f32)).astype(bf16)
        for move in started((latent_new, rope_new), outs, arrived):
            move.wait()


def kernel_call(body, outs, scalars, name, **options):
    vmem = pl.BlockSpec(memory_space=pltpu.VMEM)
    smem = pl.BlockSpec(memory_space=pltpu.SMEM)

    def call(*args):
        return pl.pallas_call(
            body,
            out_shape=outs,
            in_specs=[smem] * scalars + [vmem] * (len(args) - scalars),
            out_specs=jax.tree.map(lambda _: vmem, outs),
            name=name,
            **options,
            compiler_params=pltpu.CompilerParams(vmem_limit_bytes=24 * 2**20),
        )(*args)

    return call


def shape(dims, kind):
    return jax.ShapeDtypeStruct(dims, kind)


def exchanged(x, groups, axes="kv"):
    return lax.all_to_all(x, axes, 0, 0, axis_index_groups=groups, tiled=True)


def shards(
    tokens,
    w_qdown,
    w_kvdown,
    w_krope,
    q_gain,
    kv_gain,
    w_qup,
    w_kup,
    w_vup,
    out_gain,
    w_out,
    cache_latent,
    cache_rope,
    lengths,
    accepted,
    parent,
):
    w_q = jnp.transpose(w_qup, (1, 2, 0)).reshape(768, 768)
    w_k = jnp.transpose(w_kup, (1, 2, 0)).reshape(512, 512)
    w_v = jnp.transpose(w_vup, (1, 2, 0)).reshape(512, 512)
    gains = [g.reshape(-1, 128) for g in (q_gain, kv_gain, out_gain)]
    vmem = pl.BlockSpec(memory_space=pltpu.VMEM)
    smem = pl.BlockSpec(memory_space=pltpu.SMEM)
    hbm = pl.BlockSpec(memory_space=pltpu.HBM)
    sources = (lengths, accepted, parent, tokens.T, w_qdown, w_kvdown, w_krope, cache_latent, cache_rope)
    sources = [pltpu.with_memory_space_constraint(a, pltpu.HBM) for a in sources]
    table = shape((40, 128), f32)
    block, cosine, sine, reach = pl.pallas_call(
        project_body,
        out_shape=(shape((16, 8, 1920), bf16), table, table, shape((32, 128), f32)),
        in_specs=[hbm] * 9,
        out_specs=(vmem,) * 4,
        scratch_shapes=[pltpu.SMEM(a.shape, a.dtype) for a in sources[:3]]
        + [pltpu.VMEM(a.shape, a.dtype) for a in sources[3:]]
        + [pltpu.SemaphoreType.DMA((9,))],
        name="project",
        compiler_params=pltpu.CompilerParams(vmem_limit_bytes=24 * 2**20),
    )(*sources)
    block = exchanged(block, BLOCK)
    busy = pl.CostEstimate(flops=8_000_000_000, bytes_accessed=2_000_000, transcendentals=0)
    block_sum = kernel_call(
        block_sum_body, shape((16, 8, 768), bf16), 0, "block_sum", cost_estimate=busy
    )
    ring = exchanged(block_sum(block), RING)
    outs = (shape((672, 256), bf16), shape((128, 128), bf16))
    normalize = kernel_call(normalize_body, outs, 0, "normalize")
    own, key_rope = normalize(ring, block, cosine, sine, gains[0], gains[1], w_out.T)
    other = lax.ppermute(own, "tp", [(0, 1), (1, 0)])
    outs = (shape((4, 32, 512), bf16), shape((4, 32, 32), bf16))
    parts, fresh, *kept = pl.pallas_call(
        attend_body,
        out_shape=(shape((16, 4, 640), bf16), shape((16, 640), bf16), *outs),
        in_specs=[vmem] * 11,
        out_specs=(vmem,) * 2 + (hbm,) * 2,
        scratch_shapes=[pltpu.SemaphoreType.DMA((2,))],
        name="attend",
        compiler_params=pltpu.CompilerParams(vmem_limit_bytes=24 * 2**20),
    )(own, other, key_rope, cosine, sine, reach, w_q, w_k, w_v, cache_latent, cache_rope)
    parts = exchanged(parts, RING)
    parts = kernel_call(flat_body, shape((8, 16, 896), bf16), 0, "flat")(parts, fresh, gains[2])
    parts = exchanged(parts, ROW, ("kv", "tp"))
    mixed, latent_out, rope_out = pl.pallas_call(
        output_body,
        out_shape=(shape((32, 64), bf16), *outs),
        in_specs=[vmem] * 6 + [hbm] * 2,
        out_specs=(vmem, hbm, hbm),
        input_output_aliases={6: 1, 7: 2},
        scratch_shapes=[pltpu.VMEM(a.shape, a.dtype) for a in outs]
        + [pltpu.SemaphoreType.DMA((2,))],
        name="output",
        compiler_params=pltpu.CompilerParams(vmem_limit_bytes=24 * 2**20),
    )(parts, own, other, reach, cache_latent, cache_rope, *kept)
    return (mixed.T, latent_out, rope_out)


def solution(mesh):
    in_specs = (
        P("dp", "kv"),
        P("kv", None),
        P("kv", None),
        P("kv", None),
        P(),
        P(),
        P(None, "tp", None),
        P(None, "tp", None),
        P(None, "tp", None),
        P("tp"),
        P("tp", "kv"),
        P("dp", "kv", None),
        P("dp", "kv", None),
        P("dp"),
        P("dp"),
        P("dp", None),
    )
    out_specs = (P("dp", "kv"), P("dp", "kv", None), P("dp", "kv", None))
    return jax.shard_map(
        shards, mesh=mesh, in_specs=in_specs, out_specs=out_specs, check_vma=False
    )
```

time: 264 us -> 80.9 us (0.31)
  waiting for transfers between devices: 103 us -> 1.26 us
  blocking collectives: 96.5 us -> 70.9 us
  starting transfers between devices: 19.4 us -> 3.17 us
  between operations: 16.2 us -> 0.74 us
  local copies, waits for them, and re-layouts: 13 us -> 0.05 us
  matrix products: 9.06 us -> 0 us
  other arithmetic: 6.44 us -> 0 us
  Pallas kernels: 0 us -> 4.51 us
    all_gather x1 -> x0, waiting for transfers between devices: 81.7 us -> none  [gathered_once(): both, at, found = (lax.all_gather(jnp.concatenate(lines), axis), 0, {})]
    all_gather x2 -> x0, blocking collectives: 79.9 us -> none  [the longest x1 69.5 us: side_by_side(): result = lax.all_gather(both, axis, axis=dim, tiled=True)]
    all_to_all x1 -> x4, blocking collectives: 16.5 us -> 70.9 us  [exchanged(): return lax.all_to_all(x, axes, 0, 0, axis_index_groups=groups, tiled=True)]
    all_to_all x1 -> x0, waiting for transfers between devices: 21.4 us -> none  [sent_and_summed(): parts = lax.all_to_all(in_blocks(shard, dim, peers), axis, 0, 0, tiled=True)]
    all_to_all x1 -> x0, starting transfers between devices: 19.4 us -> none  [sent_and_summed(): parts = lax.all_to_all(in_blocks(shard, dim, peers), axis, 0, 0, tiled=True)]
    dot_general x16 -> x0, matrix products: 9.06 us -> none  [the longest x2 1.43 us: to_values(): return jnp.einsum('sphr,rhv->sphv', blend, w_vup.astype(jnp.float32))]
    pallas_call x0 -> x6, Pallas kernels: none -> 4.51 us  [the longest x1 1.61 us: shards(): pl.pallas_call(project_body, out_shape=(shape((16, 8, 1920), bf16), table...]
    unnamed x63 -> x18, local copies, waits for them, and re-layouts: 4.07 us -> 0.05 us
  transfers between devices with their start and end apart: 2 -> 1, of which waited for: 2 -> 1; matrix products, arithmetic and copies ran while one was open for 2% -> 0% of each run, Pallas kernels for 0% -> 0%
where the time goes in v1:
time: 80.9 us; the launch traced here: 80.6 us
  blocking collectives  70.9 us (88%)
  Pallas kernels  4.51 us (6%)
  starting transfers between devices  3.17 us (4%)
  waiting for transfers between devices  1.26 us (2%)
    all_to_all x4, blocking collectives, exchanged(): return lax.all_to_all(x, axes, 0, 0, axis_index_groups=groups, tiled=True)  70.9 us
    ppermute x1, starting transfers between devices, shards(): other = lax.ppermute(own, 'tp', [(0, 1), (1, 0)])  3.17 us
  transfers between devices with their start and end apart: 1, of which 1 were waited for; matrix products, arithmetic and copies ran while one was open for 0% of the time, Pallas kernels for 0%

profile of v1, /device:TPU:1, one launch (start us, length us, event | category | flops | bytes accessed | tf_op | source)
XLA Modules:
  0.0 80.6 jit_solution(5216583574233528332)
XLA Ops:
  0.6 1.6 %project.1 = (bf16[16,8,1920]{2,1,0:T(8,128)(2,1)S(1)}, f32[40,128]{1,0:T(8,128)S(1)}, f32[40,128]{1,0:T(8,128)S(1)}, f32[32,128]{1,0:T(8,128)S(1)}) custom-call(s32[4]{0:T(128)} %refs_0_.2, s32[4]{0:T(128)} %refs_1_.2, s32[4,16]{1,0:T(4,128)} %refs_2_.1, bf16[32,64]{1,0:T(8,128)(2,1)} %bitcast.22, bf16[32,768]{1,0:T(8,128)(2,1)} %refs_4_.1, ...), custom_call_target="tpu_custom_call" | custom-call | tf_op jit(solution)/shard_map/project/pallas_call | solution.py:404
  2.3 20.4 %all_to_all.20.parts.block = bf16[16,8,1920]{2,1,0:T(8,128)(2,1)S(1)} all-to-all(bf16[16,8,1920]{2,1,0:T(8,128)(2,1)S(1)} %get-tuple-element.16), channel_id=1, replica_groups={{20,22,16,18,28,30,24,26,12,14,8,10,4,6,0,2},{52,54,48,50,60,62,56,58,4..., dimensions={0} | all-to-all | bytes 983040 | tf_op jit(solution)/shard_map/all_to_all | solution.py:373
  22.7 0.0 copy-start.5
  22.7 0.0 copy-start.6
  22.7 0.0 copy-start.7
  22.7 0.0 copy-start
  22.7 0.0 copy-start.3
  22.7 0.2 block_sum.1
  22.9 0.0 copy-start.1
  22.9 0.0 copy-start.2
  22.9 0.0 copy-start.4
  23.0 25.4 %all_to_all.21.ring = bf16[16,8,768]{2,1,0:T(8,128)(2,1)S(1)} all-to-all(bf16[16,8,768]{2,1,0:T(8,128)(2,1)S(1)} %block_sum.1), channel_id=1, replica_groups={{68,76,84,92,108,100,116,124,20,28,12,4,52,60,44,36},{70,78,86,94,110,1..., dimensions={0} | all-to-all | bytes 393216 | tf_op jit(solution)/shard_map/all_to_all | solution.py:373
  48.4 0.0 copy-done.5
  48.4 0.0 copy-done.6
  48.4 0.0 copy-done.7
  48.4 0.1 normalize.1
  48.5 3.2 %collective-permute-start = (bf16[672,256]{1,0:T(8,128)(2,1)S(1)}, bf16[672,256]{1,0:T(8,128)(2,1)S(1)}, u32[]{:S(2)}, u32[]{:S(2)}) collective-permute-start(bf16[672,256]{1,0:T(8,128)(2,1)S(1)} %get-tuple-element.19.own), channel_id=1, source_target_pairs={{0,1},{1,0},{2,3},{3,2},{4,5},{5,4},{6,7},{7,6},{8,9},{9,8},{10,11... | collective-permute-start | bytes 1032200 | tf_op jit(solution)/shard_map/ppermute | solution.py:424
  51.7 1.3 %collective-permute-done.other = bf16[672,256]{1,0:T(8,128)(2,1)S(1)} collective-permute-done((bf16[672,256]{1,0:T(8,128)(2,1)S(1)}, bf16[672,256]{1,0:T(8,128)(2,1)S(1)}, u32[]{:S(2)}, u32[]{:S(2)}) %collective-permute-start) | collective-permute-done | bytes 344096 | tf_op jit(solution)/shard_map/ppermute | solution.py:424
  52.9 0.0 copy-done
  52.9 0.0 copy-done.3
  52.9 0.0 copy-done.1
  52.9 0.0 copy-done.2
  53.0 0.0 copy-done.4
  53.0 0.0 copy-start.8
  53.0 1.5 %attend.1 = (bf16[16,4,640]{2,1,0:T(4,128)(2,1)S(1)}, bf16[16,640]{1,0:T(8,128)(2,1)S(1)}, bf16[4,32,512]{2,1,0:T(8,128)(2,1)}, bf16[4,32,32]{2,1,0:T(8,128)(2,1)}) custom-call(bf16[672,256]{1,0:T(8,128)(2,1)S(1)} %get-tuple-element.19.own, bf16[672,256]{1,0:T(8,128)(2,1)S(1)} %collective-permute-done.other, ...), custom_call_target="tpu_custom_call" | custom-call | tf_op jit(solution)/shard_map/attend/pallas_call | solution.py:426
  54.5 16.0 %all_to_all.22.parts = bf16[16,4,640]{2,1,0:T(4,128)(2,1)S(1)} all-to-all(bf16[16,4,640]{2,1,0:T(4,128)(2,1)S(1)} %get-tuple-element.22), channel_id=1, replica_groups={{68,76,84,92,108,100,116,124,20,28,12,4,52,60,44,36},{70,78,86,94,110,1..., dimensions={0} | all-to-all | bytes 163840 | tf_op jit(solution)/shard_map/all_to_all | solution.py:373
  70.5 0.0 copy-done.8
  70.5 0.3 flat.1
  70.7 9.1 %all_to_all.23.parts = bf16[8,16,896]{2,1,0:T(8,128)(2,1)S(1)} all-to-all(bf16[8,16,896]{2,1,0:T(8,128)(2,1)S(1)} %flat.1), channel_id=1, replica_groups={{20,21,22,23,16,17,18,19},{28,29,30,31,24,25,26,27},{12,13,14,15,8,9,10..., dimensions={0} | all-to-all | bytes 458752 | tf_op jit(solution)/shard_map/all_to_all | solution.py:373
  79.8 0.8 output.1
Async XLA Ops:
  22.7 25.7 %copy-start.5 = (bf16[512,32]{0,1:T(8,128)(2,1)S(1)}, bf16[512,32]{0,1:T(8,128)(2,1)}, u32[]{:S(2)}) copy-start(bf16[512,32]{0,1:T(8,128)(2,1)} %param.26) | copy-start | bytes 98308
  22.7 25.7 %copy-start.6 = (bf16[768]{0:T(1024)(128)(2,1)S(1)}, bf16[768]{0:T(1024)(128)(2,1)}, u32[]{:S(2)}) copy-start(bf16[768]{0:T(1024)(128)(2,1)} %param.20) | copy-start | bytes 4612
  22.7 25.7 %copy-start.7 = (bf16[512]{0:T(512)(128)(2,1)S(1)}, bf16[512]{0:T(512)(128)(2,1)}, u32[]{:S(2)}) copy-start(bf16[512]{0:T(512)(128)(2,1)} %param.21) | copy-start | bytes 3076
  22.7 30.2 %copy-start = (bf16[768,8,96]{0,2,1:T(8,128)(2,1)S(1)}, bf16[768,8,96]{0,2,1:T(8,128)(2,1)}, u32[]{:S(2)}) copy-start(bf16[768,8,96]{0,2,1:T(8,128)(2,1)} %param.22) | copy-start | bytes 3538948
  22.7 30.2 %copy-start.3 = (bf16[512,8,64]{0,2,1:T(8,128)(2,1)S(1)}, bf16[512,8,64]{0,2,1:T(8,128)(2,1)}, u32[]{:S(2)}) copy-start(bf16[512,8,64]{0,2,1:T(8,128)(2,1)} %param.24) | copy-start | bytes 1572868
  22.9 30.0 %copy-start.1 = (bf16[4,32,512]{2,1,0:T(8,128)(2,1)S(1)}, bf16[4,32,512]{2,1,0:T(8,128)(2,1)}, u32[]{:S(2)}) copy-start(bf16[4,32,512]{2,1,0:T(8,128)(2,1)} %latent.1) | copy-start | bytes 393220
  22.9 30.0 %copy-start.2 = (bf16[512,8,64]{0,2,1:T(8,128)(2,1)S(1)}, bf16[512,8,64]{0,2,1:T(8,128)(2,1)}, u32[]{:S(2)}) copy-start(bf16[512,8,64]{0,2,1:T(8,128)(2,1)} %param.23) | copy-start | bytes 1572868
  22.9 30.0 %copy-start.4 = (bf16[4,32,32]{2,1,0:T(8,128)(2,1)S(1)}, bf16[4,32,32]{2,1,0:T(8,128)(2,1)}, u32[]{:S(2)}) copy-start(bf16[4,32,32]{2,1,0:T(8,128)(2,1)} %rope.1) | copy-start | bytes 24580
  48.5 4.4 %collective-permute-start = (bf16[672,256]{1,0:T(8,128)(2,1)S(1)}, bf16[672,256]{1,0:T(8,128)(2,1)S(1)}, u32[]{:S(2)}, u32[]{:S(2)}) collective-permute-start(bf16[672,256]{1,0:T(8,128)(2,1)S(1)} %get-tuple-element.19.own), channel_id=1, source_target_pairs={{0,1},{1,0},{2,3},{3,2},{4,5},{5,4},{6,7},{7,6},{8,9},{9,8},{10,11... | collective-permute-start | bytes 1032200 | tf_op jit(solution)/shard_map/ppermute | solution.py:424
  53.0 17.5 %copy-start.8 = (bf16[512]{0:T(512)(128)(2,1)S(1)}, bf16[512]{0:T(512)(128)(2,1)}, u32[]{:S(2)}) copy-start(bf16[512]{0:T(512)(128)(2,1)} %param.25) | copy-start | bytes 3076

commit v2 on v1

--- a/solution.py
+++ b/solution.py
@@ -12,7 +12,7 @@
 
 
 FOUR = range(4)
-LOWS = ((2, 3, 1, 0), (2, 3, 1, 0), (0, 1, 2, 3), (1, 0, 2, 3))
+LOWS = ((2, 3, 1, 0), (3, 2, 1, 0), (0, 1, 2, 3), (1, 0, 2, 3))
 HIGHS = (2, 3, 0, 1)
 YS = (2, 3, 0, 1)
 

time: 80.9 us -> 80.9 us (level)
  no operation moved by 1% of the time
where the time goes in v2:
time: 80.9 us; the launch traced here: 80.6 us
  blocking collectives  71 us (88%)
  Pallas kernels  4.51 us (6%)
  starting transfers between devices  3.09 us (4%)
  waiting for transfers between devices  1.26 us (2%)
    all_to_all x4, blocking collectives, exchanged(): return lax.all_to_all(x, axes, 0, 0, axis_index_groups=groups, tiled=True)  71 us
    ppermute x1, starting transfers between devices, shards(): other = lax.ppermute(own, 'tp', [(0, 1), (1, 0)])  3.09 us
  transfers between devices with their start and end apart: 1, of which 1 were waited for; matrix products, arithmetic and copies ran while one was open for 0% of the time, Pallas kernels for 0%

profile of v2, /device:TPU:1, one launch (start us, length us, event | category | flops | bytes accessed | tf_op | source)
XLA Modules:
  0.0 80.6 jit_solution(10563225560752066101)
XLA Ops:
  0.6 1.6 %project.1 = (bf16[16,8,1920]{2,1,0:T(8,128)(2,1)S(1)}, f32[40,128]{1,0:T(8,128)S(1)}, f32[40,128]{1,0:T(8,128)S(1)}, f32[32,128]{1,0:T(8,128)S(1)}) custom-call(s32[4]{0:T(128)} %refs_0_.2, s32[4]{0:T(128)} %refs_1_.2, s32[4,16]{1,0:T(4,128)} %refs_2_.1, bf16[32,64]{1,0:T(8,128)(2,1)} %bitcast.22, bf16[32,768]{1,0:T(8,128)(2,1)} %refs_4_.1, ...), custom_call_target="tpu_custom_call" | custom-call | tf_op jit(solution)/shard_map/project/pallas_call | solution.py:404
  2.3 20.4 %all_to_all.20.parts.block = bf16[16,8,1920]{2,1,0:T(8,128)(2,1)S(1)} all-to-all(bf16[16,8,1920]{2,1,0:T(8,128)(2,1)S(1)} %get-tuple-element.16), channel_id=1, replica_groups={{20,22,16,18,28,30,24,26,12,14,8,10,4,6,0,2},{60,62,56,58,52,54,48,50,4..., dimensions={0} | all-to-all | bytes 983040 | tf_op jit(solution)/shard_map/all_to_all | solution.py:373
  22.7 0.0 copy-start.5
  22.7 0.0 copy-start.6
  22.7 0.0 copy-start.7
  22.7 0.0 copy-start
  22.7 0.0 copy-start.3
  22.7 0.2 block_sum.1
  22.9 0.0 copy-start.1
  22.9 0.0 copy-start.2
  22.9 0.0 copy-start.4
  23.0 25.5 %all_to_all.21.ring = bf16[16,8,768]{2,1,0:T(8,128)(2,1)S(1)} all-to-all(bf16[16,8,768]{2,1,0:T(8,128)(2,1)S(1)} %block_sum.1), channel_id=1, replica_groups={{68,76,84,92,108,100,116,124,20,28,12,4,60,52,44,36},{70,78,86,94,110,1..., dimensions={0} | all-to-all | bytes 393216 | tf_op jit(solution)/shard_map/all_to_all | solution.py:373
  48.4 0.0 copy-done.5
  48.4 0.0 copy-done.6
  48.4 0.0 copy-done.7
  48.4 0.1 normalize.1
  48.6 3.1 %collective-permute-start = (bf16[672,256]{1,0:T(8,128)(2,1)S(1)}, bf16[672,256]{1,0:T(8,128)(2,1)S(1)}, u32[]{:S(2)}, u32[]{:S(2)}) collective-permute-start(bf16[672,256]{1,0:T(8,128)(2,1)S(1)} %get-tuple-element.19.own), channel_id=1, source_target_pairs={{0,1},{1,0},{2,3},{3,2},{4,5},{5,4},{6,7},{7,6},{8,9},{9,8},{10,11... | collective-permute-start | bytes 1032200 | tf_op jit(solution)/shard_map/ppermute | solution.py:424
  51.7 1.3 %collective-permute-done.other = bf16[672,256]{1,0:T(8,128)(2,1)S(1)} collective-permute-done((bf16[672,256]{1,0:T(8,128)(2,1)S(1)}, bf16[672,256]{1,0:T(8,128)(2,1)S(1)}, u32[]{:S(2)}, u32[]{:S(2)}) %collective-permute-start) | collective-permute-done | bytes 344096 | tf_op jit(solution)/shard_map/ppermute | solution.py:424
  52.9 0.0 copy-done
  52.9 0.0 copy-done.3
  52.9 0.0 copy-done.1
  52.9 0.0 copy-done.2
  53.0 0.0 copy-done.4
  53.0 0.0 copy-start.8
  53.0 1.5 %attend.1 = (bf16[16,4,640]{2,1,0:T(4,128)(2,1)S(1)}, bf16[16,640]{1,0:T(8,128)(2,1)S(1)}, bf16[4,32,512]{2,1,0:T(8,128)(2,1)}, bf16[4,32,32]{2,1,0:T(8,128)(2,1)}) custom-call(bf16[672,256]{1,0:T(8,128)(2,1)S(1)} %get-tuple-element.19.own, bf16[672,256]{1,0:T(8,128)(2,1)S(1)} %collective-permute-done.other, ...), custom_call_target="tpu_custom_call" | custom-call | tf_op jit(solution)/shard_map/attend/pallas_call | solution.py:426
  54.5 16.0 %all_to_all.22.parts = bf16[16,4,640]{2,1,0:T(4,128)(2,1)S(1)} all-to-all(bf16[16,4,640]{2,1,0:T(4,128)(2,1)S(1)} %get-tuple-element.22), channel_id=1, replica_groups={{68,76,84,92,108,100,116,124,20,28,12,4,60,52,44,36},{70,78,86,94,110,1..., dimensions={0} | all-to-all | bytes 163840 | tf_op jit(solution)/shard_map/all_to_all | solution.py:373
  70.4 0.0 copy-done.8
  70.4 0.3 flat.1
  70.7 9.1 %all_to_all.23.parts = bf16[8,16,896]{2,1,0:T(8,128)(2,1)S(1)} all-to-all(bf16[8,16,896]{2,1,0:T(8,128)(2,1)S(1)} %flat.1), channel_id=1, replica_groups={{20,21,22,23,16,17,18,19},{28,29,30,31,24,25,26,27},{12,13,14,15,8,9,10..., dimensions={0} | all-to-all | bytes 458752 | tf_op jit(solution)/shard_map/all_to_all | solution.py:373
  79.8 0.8 output.1
Async XLA Ops:
  22.7 25.8 %copy-start.5 = (bf16[512,32]{0,1:T(8,128)(2,1)S(1)}, bf16[512,32]{0,1:T(8,128)(2,1)}, u32[]{:S(2)}) copy-start(bf16[512,32]{0,1:T(8,128)(2,1)} %param.26) | copy-start | bytes 98308
  22.7 25.8 %copy-start.6 = (bf16[768]{0:T(1024)(128)(2,1)S(1)}, bf16[768]{0:T(1024)(128)(2,1)}, u32[]{:S(2)}) copy-start(bf16[768]{0:T(1024)(128)(2,1)} %param.20) | copy-start | bytes 4612
  22.7 25.8 %copy-start.7 = (bf16[512]{0:T(512)(128)(2,1)S(1)}, bf16[512]{0:T(512)(128)(2,1)}, u32[]{:S(2)}) copy-start(bf16[512]{0:T(512)(128)(2,1)} %param.21) | copy-start | bytes 3076
  22.7 30.2 %copy-start = (bf16[768,8,96]{0,2,1:T(8,128)(2,1)S(1)}, bf16[768,8,96]{0,2,1:T(8,128)(2,1)}, u32[]{:S(2)}) copy-start(bf16[768,8,96]{0,2,1:T(8,128)(2,1)} %param.22) | copy-start | bytes 3538948
  22.7 30.2 %copy-start.3 = (bf16[512,8,64]{0,2,1:T(8,128)(2,1)S(1)}, bf16[512,8,64]{0,2,1:T(8,128)(2,1)}, u32[]{:S(2)}) copy-start(bf16[512,8,64]{0,2,1:T(8,128)(2,1)} %param.24) | copy-start | bytes 1572868
  22.9 30.0 %copy-start.1 = (bf16[4,32,512]{2,1,0:T(8,128)(2,1)S(1)}, bf16[4,32,512]{2,1,0:T(8,128)(2,1)}, u32[]{:S(2)}) copy-start(bf16[4,32,512]{2,1,0:T(8,128)(2,1)} %latent.1) | copy-start | bytes 393220
  22.9 30.0 %copy-start.2 = (bf16[512,8,64]{0,2,1:T(8,128)(2,1)S(1)}, bf16[512,8,64]{0,2,1:T(8,128)(2,1)}, u32[]{:S(2)}) copy-start(bf16[512,8,64]{0,2,1:T(8,128)(2,1)} %param.23) | copy-start | bytes 1572868
  22.9 30.0 %copy-start.4 = (bf16[4,32,32]{2,1,0:T(8,128)(2,1)S(1)}, bf16[4,32,32]{2,1,0:T(8,128)(2,1)}, u32[]{:S(2)}) copy-start(bf16[4,32,32]{2,1,0:T(8,128)(2,1)} %rope.1) | copy-start | bytes 24580
  48.6 4.4 %collective-permute-start = (bf16[672,256]{1,0:T(8,128)(2,1)S(1)}, bf16[672,256]{1,0:T(8,128)(2,1)S(1)}, u32[]{:S(2)}, u32[]{:S(2)}) collective-permute-start(bf16[672,256]{1,0:T(8,128)(2,1)S(1)} %get-tuple-element.19.own), channel_id=1, source_target_pairs={{0,1},{1,0},{2,3},{3,2},{4,5},{5,4},{6,7},{7,6},{8,9},{9,8},{10,11... | collective-permute-start | bytes 1032200 | tf_op jit(solution)/shard_map/ppermute | solution.py:424
  53.0 17.5 %copy-start.8 = (bf16[512]{0:T(512)(128)(2,1)S(1)}, bf16[512]{0:T(512)(128)(2,1)}, u32[]{:S(2)}) copy-start(bf16[512]{0:T(512)(128)(2,1)} %param.25) | copy-start | bytes 3076
